TPU v7x, 32 devices: a whole 2x2x4 slice. The times are simulated.
32 devices in a mesh: sp: 16 (over z, y, x), tp: 2 (over core).
Axes of the slice: x: 2, y: 2, z: 4, core: 2. Of those that a mesh axis runs over, the one named last changes fastest.
Arguments:
- tokens: bfloat16 [2048, 4096], P('sp'), may hold values from -6 to 6
- norm_gain: float32 [4096], replicated, may hold values from 0.1 to 1.9
- w_query: bfloat16 [4096, 2048], P('sp', 'tp'), may hold values from -1 to 1
- w_key: bfloat16 [4096, 512], P('sp', 'tp'), may hold values from -1 to 1
- w_value: bfloat16 [4096, 512], P('sp', 'tp'), may hold values from -0.09375 to 0.09375
- w_state_in: bfloat16 [4096, 2048], P('sp', 'tp'), may hold values from -0.09375 to 0.09375
- sink_logit: float32 [32], P('tp'), may hold values from 2 to 6
- decay_rate: float32 [128, 64], P('tp'), may hold values from 0.0002 to 4
- rotation: float32 [128, 64], P('tp'), may hold values from 1 to 60
- log_step: float32 [128], P('tp'), may hold values from -5.3 to -3
- in_re: float32 [128, 64, 16], P('tp'), may hold values from -1.5 to 1.5
- in_im: float32 [128, 64, 16], P('tp'), may hold values from -1.5 to 1.5
- out_re: float32 [128, 16, 64], P('tp'), may hold values from -0.75 to 0.75
- out_im: float32 [128, 16, 64], P('tp'), may hold values from -0.75 to 0.75
- skip_gain: float32 [2048], P('tp'), may hold values from -4 to 4
- w_attn_out: bfloat16 [2048, 4096], P('tp', 'sp'), may hold values from -0.5 to 0.5
- w_state_out: bfloat16 [2048, 4096], P('tp', 'sp'), may hold values from -0.125 to 0.125
- out_gain: float32 [4096], replicated, may hold values from 0.1 to 1.9
Outputs:
- mixed: bfloat16 [2048, 4096], P(('sp', 'tp'))
All inputs are finite; a program needn't handle non-finite values.
Results may differ from a plain program's by a relative error of at most 0.015.
The roundings to bfloat16 on the way count: a program that leaves them out, or rounds other values in their place, can miss the bound.
Values may be sent and summed in bfloat16 or wider, within the bound.
No kernel may reach another device: no remote copies, remote signals or barrier semaphores. Data moves between devices by JAX's collectives and lax.ppermute only.
A program may use at most 128 MiB of HBM per device.

v0:
```python
import math

import jax
import jax.numpy as jnp
from jax import lax
from jax.sharding import PartitionSpec as P

HEAD = 64
WINDOW = 128


epsilon = 1e-06
rotary_base = 500000.0


def carried_in(value, axis, join, neutral):
    count, mine = (lax.axis_size(axis), lax.axis_index(axis))
    pieces = jax.tree.map(lambda part: lax.all_gather(part, axis), value)
    so_far = jax.tree.map(
        lambda part, zero: jnp.full_like(part, 0) + jnp.asarray(zero, part.dtype), value, neutral
    )

    def turn(position, so_far):
        longer = join(so_far, jax.tree.map(lambda part: part[position], pieces))
        return jax.tree.map(lambda new, old: jnp.where(position < mine, new, old), longer, so_far)

    return lax.fori_loop(0, count - 1, turn, so_far)


def passed_along(value, axis, by):
    size = lax.axis_size(axis)
    pairs = [(i, i + by) for i in range(size) if 0 <= i + by < size]
    return lax.ppermute(value, axis, pairs)


def rotate(heads_block, positions):
    head_width = heads_block.shape[-1]
    half_width = head_width // 2
    frequency = rotary_base ** (-(jnp.arange(half_width, dtype=jnp.float32) * 2.0 / head_width))
    angles = positions.astype(jnp.float32)[:, None] * frequency[None, :]
    cosine = jnp.cos(angles)[:, None, :]
    sine_part = jnp.sin(angles)[:, None, :]
    lower_half = heads_block[..., :half_width]
    upper_half = heads_block[..., half_width:]
    return jnp.concatenate(
        [
            lower_half * cosine - upper_half * sine_part,
            upper_half * cosine + lower_half * sine_part,
        ],
        axis=-1,
    )


def shape_heads(query_sum, key_sum, value_sum, positions, head_width):
    row_count = query_sum.shape[0]
    kv_heads = key_sum.shape[1] // head_width
    group_size = query_sum.shape[1] // key_sum.shape[1]
    queries = rotate(
        query_sum.reshape(row_count, kv_heads * group_size, head_width), positions
    ).astype(jnp.bfloat16)
    queries = queries.reshape(row_count, kv_heads, group_size, head_width)
    key_rows = rotate(key_sum.reshape(row_count, kv_heads, head_width), positions).astype(
        jnp.bfloat16
    )
    key_rows = key_rows.reshape(row_count, kv_heads * head_width)
    value_rows = value_sum.astype(jnp.bfloat16)
    return (queries, key_rows, value_rows)


def band_attention(queries, key_rows, value_rows, sink_logit, first_row, window):
    row_count, kv_heads, group_size, head_width = queries.shape
    blocks = row_count // window
    query_blocks = queries.reshape(blocks, window, kv_heads, group_size, head_width)
    key_blocks = jnp.concatenate(
        [
            key_rows[:row_count].reshape(blocks, window, kv_heads, head_width),
            key_rows[window:].reshape(blocks, window, kv_heads, head_width),
        ],
        axis=1,
    )
    value_blocks = jnp.concatenate(
        [
            value_rows[:row_count].reshape(blocks, window, kv_heads, head_width),
            value_rows[window:].reshape(blocks, window, kv_heads, head_width),
        ],
        axis=1,
    )
    scores = jnp.einsum(
        "bqkgd,bskd->bkgqs", query_blocks, key_blocks, preferred_element_type=jnp.float32
    ) / math.sqrt(head_width)
    block_start = jnp.arange(blocks, dtype=jnp.int32)[:, None, None] * window
    query_at = first_row + block_start + jnp.arange(window, dtype=jnp.int32)[None, :, None]
    key_at = (
        first_row - window + block_start + jnp.arange(2 * window, dtype=jnp.int32)[None, None, :]
    )
    offset_gap = query_at - key_at
    visible = (offset_gap >= 0) & (offset_gap < window) & (key_at >= 0)
    scores = jnp.where(visible[:, None, None, :, :], scores, -jnp.inf)
    sink_value = sink_logit.reshape(1, kv_heads, group_size, 1, 1)
    top_score = jnp.maximum(jnp.max(scores, axis=-1, keepdims=True), sink_value)
    exponent = jnp.exp(scores - top_score)
    totals = jnp.sum(exponent, axis=-1, keepdims=True) + jnp.exp(sink_value - top_score)
    weights = (exponent / totals).astype(jnp.bfloat16)
    attended = jnp.einsum(
        "bkgqs,bskd->bqkgd", weights, value_blocks, preferred_element_type=jnp.float32
    )
    return attended.reshape(row_count, kv_heads * group_size * head_width).astype(jnp.bfloat16)


def discretize(decay_rate, rotation, log_step, in_re, in_im):
    time_step = jnp.exp(log_step)[:, None]
    lambda_re = -decay_rate
    modulus = jnp.exp(lambda_re * time_step)
    pole_re = modulus * jnp.cos(rotation * time_step)
    pole_im = modulus * jnp.sin(rotation * time_step)
    minus_one = pole_re - 1.0
    denominator = lambda_re * lambda_re + rotation * rotation
    factor_re = ((minus_one * lambda_re + pole_im * rotation) / denominator)[..., None]
    factor_im = ((pole_im * lambda_re - minus_one * rotation) / denominator)[..., None]
    drive_re = factor_re * in_re - factor_im * in_im
    drive_im = factor_re * in_im + factor_im * in_re
    return (pole_re, pole_im, drive_re, drive_im)


def chain_link(earlier, later):
    early_are, early_aim, early_bre, early_bim = earlier
    late_are, late_aim, late_bre, late_bim = later
    return (
        late_are * early_are - late_aim * early_aim,
        late_are * early_aim + late_aim * early_are,
        late_are * early_bre - late_aim * early_bim + late_bre,
        late_are * early_bim + late_aim * early_bre + late_bim,
    )


def local_states(inputs, pole_re, pole_im, drive_re, drive_im):
    row_count = inputs.shape[0]
    groups, states, group_width = drive_re.shape
    channel_values = inputs.astype(jnp.float32).reshape(row_count, groups, group_width)
    push_re = jnp.einsum(
        "tgh,gph->tgp", channel_values, drive_re, precision=lax.Precision.HIGHEST
    ).reshape(row_count, groups * states)
    push_im = jnp.einsum(
        "tgh,gph->tgp", channel_values, drive_im, precision=lax.Precision.HIGHEST
    ).reshape(row_count, groups * states)
    decay_re = jnp.broadcast_to(pole_re.reshape(1, groups * states), push_re.shape)
    decay_im = jnp.broadcast_to(pole_im.reshape(1, groups * states), push_im.shape)
    return lax.associative_scan(chain_link, (decay_re, decay_im, push_re, push_im), axis=0)


def apply_carry(running, carry_re, carry_im):
    power_re, power_im, own_re, own_im = running
    return (
        own_re + power_re * carry_re - power_im * carry_im,
        own_im + power_re * carry_im + power_im * carry_re,
    )


def read_out(inputs, state_re, state_im, out_re, out_im, skip_gain):
    row_count = inputs.shape[0]
    groups, group_width, states = out_re.shape
    grid_re = state_re.reshape(row_count, groups, states)
    grid_im = state_im.reshape(row_count, groups, states)
    summed = jnp.einsum(
        "tgp,ghp->tgh", grid_re, out_re, precision=lax.Precision.HIGHEST
    ) - jnp.einsum("tgp,ghp->tgh", grid_im, out_im, precision=lax.Precision.HIGHEST)
    summed = summed.reshape(row_count, groups * group_width) + skip_gain * inputs.astype(
        jnp.float32
    )
    return jax.nn.gelu(summed).astype(jnp.bfloat16)


def chain_in(power_re, power_im, end_re, end_im):
    identity = (
        jnp.ones_like(power_re),
        jnp.zeros_like(power_im),
        jnp.zeros_like(end_re),
        jnp.zeros_like(end_im),
    )
    before = carried_in((power_re, power_im, end_re, end_im), "sp", chain_link, identity)
    return (before[2], before[3])


def state_branch(inputs, decay_rate, rotation, log_step, in_re, in_im, out_re, out_im, skip_gain):
    pole_re, pole_im, drive_re, drive_im = discretize(decay_rate, rotation, log_step, in_re, in_im)
    running = local_states(inputs, pole_re, pole_im, drive_re, drive_im)
    carry_re, carry_im = chain_in(running[0][-1], running[1][-1], running[2][-1], running[3][-1])
    state_re, state_im = apply_carry(running, carry_re, carry_im)
    return read_out(inputs, state_re, state_im, out_re, out_im, skip_gain)


def earlier_window(key_rows, value_rows):
    joined = jnp.concatenate([key_rows, value_rows], axis=1)
    prior = passed_along(joined, "sp", 1)
    return jnp.concatenate([prior, joined], axis=0)


def make_adder(normed_cols):

    def add_pieces(carried, weight_pieces, row_start):
        updated = []
        for running_total, weight_piece in zip(carried, weight_pieces):
            product = lax.dot_general(
                normed_cols,
                weight_piece,
                (((0,), (0,)), ((), ())),
                preferred_element_type=jnp.float32,
            )
            updated.append(product)
        return tuple(updated)

    return add_pieces


def body(
    tokens,
    norm_gain,
    w_query,
    w_key,
    w_value,
    w_state_in,
    sink_logit,
    decay_rate,
    rotation,
    log_step,
    in_re,
    in_im,
    out_re,
    out_im,
    skip_gain,
    w_attn_out,
    w_state_out,
    out_gain,
):
    row_count = tokens.shape[0]
    window = WINDOW
    head_width = HEAD
    wide_tokens = tokens.astype(jnp.float32)
    normed = (
        wide_tokens
        * lax.rsqrt(jnp.mean(wide_tokens * wide_tokens, axis=-1, keepdims=True) + epsilon)
        * norm_gain
    ).astype(jnp.bfloat16)
    first_row = lax.axis_index("sp") * row_count
    positions = first_row + jnp.arange(row_count, dtype=jnp.int32)
    add_pieces = make_adder(jnp.transpose(normed))

    def empty_like(weight_shard):
        return jnp.zeros((row_count, weight_shard.shape[1]), jnp.float32)

    query_sum, key_sum, value_sum, input_sum = add_pieces(
        (empty_like(w_query), empty_like(w_key), empty_like(w_value), empty_like(w_state_in)),
        (
            lax.all_gather(w_query, "sp", axis=0, tiled=True),
            lax.all_gather(w_key, "sp", axis=0, tiled=True),
            lax.all_gather(w_value, "sp", axis=0, tiled=True),
            lax.all_gather(w_state_in, "sp", axis=0, tiled=True),
        ),
        jnp.int32(0),
    )
    queries, key_rows, value_rows = shape_heads(
        query_sum, key_sum, value_sum, positions, head_width
    )
    joined_rows = earlier_window(key_rows, value_rows)
    inputs = input_sum.astype(jnp.bfloat16)
    mixed_state = state_branch(
        inputs, decay_rate, rotation, log_step, in_re, in_im, out_re, out_im, skip_gain
    )
    kv_width = key_rows.shape[1]
    kv_heads = kv_width // head_width
    all_keys = joined_rows[:, :kv_width].reshape(window + row_count, kv_heads, head_width)
    all_values = joined_rows[:, kv_width:].reshape(window + row_count, kv_heads, head_width)
    attended = band_attention(queries, all_keys, all_values, sink_logit, first_row, window)
    attn_rows, state_rows = (
        lax.all_gather(w_attn_out, "sp", axis=1, tiled=True),
        lax.all_gather(w_state_out, "sp", axis=1, tiled=True),
    )
    projected = lax.psum_scatter(
        (
            jnp.dot(attended, attn_rows, preferred_element_type=jnp.float32)
            + jnp.dot(mixed_state, state_rows, preferred_element_type=jnp.float32)
        ).astype(jnp.bfloat16),
        "tp",
        scatter_dimension=0,
        tiled=True,
    ).astype(jnp.float32)
    row_scale = lax.rsqrt(jnp.mean(projected * projected, axis=-1, keepdims=True) + epsilon)
    return (projected * row_scale * out_gain).astype(jnp.bfloat16)


def solution(mesh):
    return jax.shard_map(
        body,
        mesh=mesh,
        in_specs=(
            P("sp", None),
            P(),
            P("sp", "tp"),
            P("sp", "tp"),
            P("sp", "tp"),
            P("sp", "tp"),
            P("tp"),
            P("tp", None),
            P("tp", None),
            P("tp"),
            P("tp", None, None),
            P("tp", None, None),
            P("tp", None, None),
            P("tp", None, None),
            P("tp"),
            P("tp", "sp"),
            P("tp", "sp"),
            P(),
        ),
        out_specs=P(("sp", "tp"), None),
        check_vma=False,
    )
```

profile of v0, /device:TPU:0, one launch (start us, length us, event | category | flops | bytes accessed | tf_op | source)
XLA Modules:
  0.0 1007.8 jit_solution(5649629984481578500)
XLA Ops:
  17.2 56.1 %all-gather.11.cloned.1.call-done = bf16[4096,256]{1,0:T(8,128)(2,1)} async-done(((bf16[256,256]{1,0:T(8,128)(2,1)}), bf16[4096,256]{1,0:T(8,128)(2,1)}) %all-gather.11.cloned.1.call-update) | async-done | bytes 2097168 | tf_op jit(solution)/shard_map/all_gather | solution.py:255
  76.1 59.2 %all-gather.13.cloned.1.call-done = bf16[4096,256]{1,0:T(8,128)(2,1)} async-done(((bf16[256,256]{1,0:T(8,128)(2,1)}), bf16[4096,256]{1,0:T(8,128)(2,1)}) %all-gather.13.cloned.1.call-update) | async-done | bytes 2097168 | tf_op jit(solution)/shard_map/all_gather | solution.py:256
  144.5 104.6 %all-gather.19.cloned.1.call-done = bf16[4096,1024]{1,0:T(8,128)(2,1)} async-done(((bf16[256,1024]{1,0:T(8,128)(2,1)}), bf16[4096,1024]{1,0:T(8,128)(2,1)}) %all-gather.19.cloned.1.call-update) | async-done | bytes 8388624 | tf_op jit(solution)/shard_map/all_gather | solution.py:257
  249.2 4.7 convolution_convert_fusion
  260.6 38.2 %slice.402 = f32[64,4096]{0,1:T(8,128)} slice(f32[128,4096]{0,1:T(8,128)S(1)} %bitcast.93), slice={[0:127:2], [0:4096:1]} | slice | bytes 2097152 | tf_op jit(solution)/shard_map/slice | solution.py:148
  298.8 41.3 %slice.405 = f32[64,4096]{0,1:T(8,128)} slice(f32[128,4096]{0,1:T(8,128)S(1)} %bitcast.94), slice={[1:128:2], [0:4096:1]} | slice | bytes 2097152 | tf_op jit(solution)/shard_map/slice | solution.py:148
  340.1 38.3 %slice.404 = f32[64,4096]{0,1:T(8,128)} slice(f32[128,4096]{0,1:T(8,128)} %bitcast.97), slice={[0:127:2], [0:4096:1]} | slice | bytes 2097152 | tf_op jit(solution)/shard_map/slice | solution.py:148
  378.4 38.9 %slice.411 = f32[64,4096]{0,1:T(8,128)} slice(f32[128,4096]{0,1:T(8,128)} %bitcast.98), slice={[1:128:2], [0:4096:1]} | slice | bytes 2097152 | tf_op jit(solution)/shard_map/slice | solution.py:148
  502.4 40.7 %slice.482 = f32[63,4096]{0,1:T(8,128)} slice(f32[128,4096]{0,1:T(8,128)S(1)} %bitcast.95), slice={[2:128:2], [0:4096:1]} | slice | bytes 2064384 | tf_op jit(solution)/shard_map/slice | solution.py:148
  543.1 50.7 %slice.500 = f32[63,4096]{0,1:T(8,128)} slice(f32[128,4096]{0,1:T(8,128)} %bitcast.99), slice={[2:128:2], [0:4096:1]} | slice | bytes 2064384 | tf_op jit(solution)/shard_map/slice | solution.py:148
  622.5 4.6 pad.223
  629.4 4.6 pad.222
  636.8 4.6 pad.220
  674.9 4.6 pad.196
  685.0 8.6 pad.229
  695.6 4.6 pad.194
  719.0 8.7 pad.228
  728.7 39.4 %all-gather.3 = f32[16,1,4096]{2,1,0:T(1,128)S(1)} all-gather(f32[1,1,4096]{2,1,0:T(1,128)S(1)} %add_bitcast_fusion), channel_id=1, replica_groups=mesh['sp'=16,'tp'=2] {'sp'}, dimensions={0}, use_global_device_ids=true | all-gather | bytes 278528 | tf_op jit(solution)/shard_map/all_gather | solution.py:18
  768.2 8.6 pad.199
  785.1 36.9 %all-gather.2 = f32[16,1,4096]{2,1,0:T(1,128)S(1)} all-gather(f32[1,1,4096]{2,1,0:T(1,128)S(1)} %add_bitcast_fusion.1), channel_id=1, replica_groups=mesh['sp'=16,'tp'=2] {'sp'}, dimensions={0}, use_global_device_ids=true | all-gather | bytes 278528 | tf_op jit(solution)/shard_map/all_gather | solution.py:18
  822.1 8.6 pad.227
  833.0 8.7 pad.226
  842.7 39.0 %all-gather.1 = f32[16,1,4096]{2,1,0:T(1,128)S(1)} all-gather(f32[1,1,4096]{2,1,0:T(1,128)S(1)} %add_bitcast_fusion.2), channel_id=1, replica_groups=mesh['sp'=16,'tp'=2] {'sp'}, dimensions={0}, use_global_device_ids=true | all-gather | bytes 278528 | tf_op jit(solution)/shard_map/all_gather | solution.py:18
  883.2 4.9 pad.224
  888.1 8.7 pad.225
  897.8 37.0 %all-gather = f32[16,1,4096]{2,1,0:T(1,128)S(1)} all-gather(f32[1,1,4096]{2,1,0:T(1,128)S(1)} %add_bitcast_fusion.3), channel_id=1, replica_groups=mesh['sp'=16,'tp'=2] {'sp'}, dimensions={0}, use_global_device_ids=true | all-gather | bytes 278528 | tf_op jit(solution)/shard_map/all_gather | solution.py:18
  935.7 15.3 %while.16 = (s32[]{:T(128)}, f32[4096]{0:T(1024)S(1)}, f32[4096]{0:T(1024)S(1)}, s32[]{:T(128)}, f32[16,4096]{1,0:T(8,128)}, /*index=5*/f32[16,4096]{1,0:T(8,128...) while((s32[]{:T(128)}, f32[4096]{0:T(1024)S(1)}, ...), condition=%wide.region_4.5_spmd.clone, body=%wide.region_3.4_spmd.clone.sunk | while | flops 49156 | bytes 262273 | solution.py:27
  951.0 9.2 multiply_add_fusion
  971.2 6.8 fusion.58
  980.4 4.8 fusion.65
  985.3 5.8 fusion
  991.1 6.2 reduce-scatter.2.cloned.1.call-done
  (482 shorter events, 254.2 us)
Async XLA Ops:
  6.5 958.7 %copy-start = (f32[64,16,64]{2,1,0:T(8,128)S(1)}, f32[64,16,64]{2,1,0:T(8,128)}, u32[]{:S(2)}) copy-start(f32[64,16,64]{2,1,0:T(8,128)} %param.32) | copy-start | bytes 786436
  6.6 66.7 %all-gather.11.cloned.1.call-start = ((), (), s32[]{:S(2)}) async-start(), calls=%async_computation.1 | async-start | bytes 2228224 | tf_op jit(solution)/shard_map/all_gather | solution.py:255
  7.3 128.0 %all-gather.13.cloned.1.call-start = ((), (), s32[]{:S(2)}) async-start(), calls=%async_computation.2 | async-start | bytes 2228224 | tf_op jit(solution)/shard_map/all_gather | solution.py:256
  8.0 241.1 %all-gather.19.cloned.1.call-start = ((), (), s32[]{:S(2)}) async-start(), calls=%async_computation.5 | async-start | bytes 8912896 | tf_op jit(solution)/shard_map/all_gather | solution.py:257
  8.8 64.5 %copy-start.101 = (f32[4096]{0:T(1024)S(1)}, f32[4096]{0:T(1024)}, u32[]{:S(2)}) copy-start(f32[4096]{0:T(1024)} %param.21) | copy-start | bytes 49156
  8.8 962.4 %all-gather.15.cloned.1.call-start = ((), (), s32[]{:S(2)}) async-start(), calls=%async_computation.3 | async-start | bytes 8912896 | tf_op jit(solution)/shard_map/all_gather | solution.py:254
  9.4 971.0 %all-gather.17.cloned.1.call-start = ((), (), s32[]{:S(2)}) async-start(), calls=%async_computation.4 | async-start | bytes 8912896 | tf_op jit(solution)/shard_map/all_gather | solution.py:275
  10.0 975.3 %all-gather.21.cloned.1.call-start = ((), (), s32[]{:S(2)}) async-start(), calls=%async_computation.6 | async-start | bytes 8912896 | tf_op jit(solution)/shard_map/all_gather | solution.py:276
  10.5 986.7 %reduce-scatter.2.cloned.1.call-start = ((), (), s32[]{:S(2)}) async-start(), calls=%async_computation.7 | async-start | bytes 1572864 | tf_op jit(solution)/shard_map/reduce_scatter | solution.py:278
  10.9 419.2 %copy-start.35 = (f32[4096]{0:T(1024)}, f32[4096]{0:T(1024)S(1)}, u32[]{:S(2)}) copy-start(f32[4096]{0:T(1024)S(1)} %broadcast_in_dim.18) | copy-start | bytes 49156
  11.0 64.9 %copy-start.61 = (f32[1,4096]{1,0:T(1,128)}, f32[1,4096]{1,0:T(1,128)S(1)}, u32[]{:S(2)}) copy-start(f32[1,4096]{1,0:T(1,128)S(1)} %broadcast_in_dim.20) | copy-start | bytes 49156
  11.1 419.1 %copy-start.38 = (f32[4096]{0:T(1024)}, f32[4096]{0:T(1024)S(1)}, u32[]{:S(2)}) copy-start(f32[4096]{0:T(1024)S(1)} %broadcast_in_dim.19) | copy-start | bytes 49156
  11.2 64.7 %copy-start.63 = (f32[1,4096]{1,0:T(1,128)}, f32[1,4096]{1,0:T(1,128)S(1)}, u32[]{:S(2)}) copy-start(f32[1,4096]{1,0:T(1,128)S(1)} %broadcast_in_dim.21) | copy-start | bytes 49156
  11.6 237.6 %copy-start.104 = (f32[128]{0:T(128)}, f32[128]{0:T(128)S(1)}, u32[]{:S(2)}) copy-start(f32[128]{0:T(128)S(1)} %add_rsqrt_fusion.1) | copy-start | bytes 1540
  16.4 120.9 %copy-start.41 = (f32[4096]{0:T(1024)}, f32[4096]{0:T(1024)S(1)}, u32[]{:S(2)}) copy-start(f32[4096]{0:T(1024)S(1)} %get-tuple-element.204) | copy-start | bytes 49156
  16.4 120.9 %copy-start.44 = (f32[4096]{0:T(1024)}, f32[4096]{0:T(1024)S(1)}, u32[]{:S(2)}) copy-start(f32[4096]{0:T(1024)S(1)} %get-tuple-element.205) | copy-start | bytes 49156
  17.2 58.7 %copy-start.65 = (f32[128,32]{0,1:T(8,128)}, f32[128,32]{0,1:T(8,128)S(1)}, u32[]{:S(2)}) copy-start(f32[128,32]{0,1:T(8,128)S(1)} %get-tuple-element.273) | copy-start | bytes 49156
  17.2 58.7 %copy-start.67 = (f32[128,32]{0,1:T(8,128)}, f32[128,32]{0,1:T(8,128)S(1)}, u32[]{:S(2)}) copy-start(f32[128,32]{0,1:T(8,128)S(1)} %get-tuple-element.274) | copy-start | bytes 49156
  75.9 61.4 %copy-start.71 = (bf16[128,4,32]{0,2,1:T(8,128)(2,1)}, bf16[128,4,32]{0,2,1:T(8,128)(2,1)S(1)}, u32[]{:S(2)}) copy-start(bf16[128,4,32]{0,2,1:T(8,128)(2,1)S(1)} %get-tuple-element.252) | copy-start | bytes 98308
  75.9 61.4 %copy-start.73 = (bf16[128,4,32]{0,2,1:T(8,128)(2,1)}, bf16[128,4,32]{0,2,1:T(8,128)(2,1)S(1)}, u32[]{:S(2)}) copy-start(bf16[128,4,32]{0,2,1:T(8,128)(2,1)S(1)} %get-tuple-element.253) | copy-start | bytes 98308
  137.4 5.7 collective-permute-start
  144.5 110.0 %copy-start.22 = (f32[64,64,16]{1,2,0:T(8,128)S(1)}, f32[64,64,16]{1,2,0:T(8,128)}, u32[]{:S(2)}) copy-start(f32[64,64,16]{1,2,0:T(8,128)} %param.30) | copy-start | bytes 786436
  543.1 50.8 %copy-start.96 = (f32[1,4096]{1,0:T(1,128)S(1)}, f32[1,4096]{1,0:T(1,128)}, u32[]{:S(2)}) copy-start(f32[1,4096]{1,0:T(1,128)} %get-tuple-element.257) | copy-start | bytes 49156
  543.1 50.9 %copy-start.57 = (f32[1,4096]{1,0:T(1,128)S(1)}, f32[1,4096]{1,0:T(1,128)}, u32[]{:S(2)}) copy-start(f32[1,4096]{1,0:T(1,128)} %get-tuple-element.194) | copy-start | bytes 49156
  543.1 50.9 %copy-start.95 = (f32[1,4096]{1,0:T(1,128)S(1)}, f32[1,4096]{1,0:T(1,128)}, u32[]{:S(2)}) copy-start(f32[1,4096]{1,0:T(1,128)} %get-tuple-element.256) | copy-start | bytes 49156
  543.1 51.0 %copy-start.32 = (f32[4,4096]{1,0:T(4,128)S(1)}, f32[4,4096]{1,0:T(4,128)}, u32[]{:S(2)}) copy-start(f32[4,4096]{1,0:T(4,128)} %pad.207) | copy-start | bytes 196612
  543.1 51.1 %copy-start.31 = (f32[4,4096]{1,0:T(4,128)S(1)}, f32[4,4096]{1,0:T(4,128)}, u32[]{:S(2)}) copy-start(f32[4,4096]{1,0:T(4,128)} %pad.205) | copy-start | bytes 196612
  543.1 51.1 %copy-start.42 = (f32[4096]{0:T(1024)S(1)}, f32[4096]{0:T(1024)}, u32[]{:S(2)}) copy-start(f32[4096]{0:T(1024)} %copy-done.41) | copy-start | bytes 49156
  543.1 51.1 %copy-start.45 = (f32[4096]{0:T(1024)S(1)}, f32[4096]{0:T(1024)}, u32[]{:S(2)}) copy-start(f32[4096]{0:T(1024)} %copy-done.44) | copy-start | bytes 49156
  543.1 51.1 %copy-start.94 = (f32[1,4096]{1,0:T(1,128)S(1)}, f32[1,4096]{1,0:T(1,128)}, u32[]{:S(2)}) copy-start(f32[1,4096]{1,0:T(1,128)} %get-tuple-element.196) | copy-start | bytes 49156
  543.1 51.3 %copy-start.93 = (f32[1,4096]{1,0:T(1,128)S(1)}, f32[1,4096]{1,0:T(1,128)}, u32[]{:S(2)}) copy-start(f32[1,4096]{1,0:T(1,128)} %get-tuple-element.195) | copy-start | bytes 49156
  888.1 62.8 %copy-start.8 = (f32[128,4096]{1,0:T(8,128)S(1)}, f32[128,4096]{1,0:T(8,128)}, u32[]{:S(2)}) copy-start(f32[128,4096]{1,0:T(8,128)} %pad.229) | copy-start | bytes 6291460
  (84 other events, 585.4 us)
Sparse Core Ops, SparseCore 0:
  10.1 63.0 all-gather.10
  76.0 59.1 all-gather.12
  138.0 111.0 all-gather.18
  251.8 110.4 all-gather.14
  364.8 132.6 all-gather.16
  500.1 132.6 all-gather.20
  991.2 6.0 reduce-scatter.1
where the time goes:
time: 1020 us; the launch traced here: 1010 us
  local copies, waits for them, and re-layouts  469 us (46%)
  waiting for transfers between devices  231 us (23%)
  blocking collectives  152 us (15%)
  other arithmetic  96.5 us (9%)
  matrix products  40 us (4%)
  between operations  15.5 us (2%)
    slice x47, local copies, waits for them, and re-layouts, local_states(): lax.associative_scan(chain_link, (decay_re, decay_im, push_re, push_im),...  306 us
    all_gather x4, blocking collectives, carried_in(): pieces = jax.tree.map(lambda part: lax.all_gather(part, axis), value)  152 us
    pad x48, local copies, waits for them, and re-layouts, local_states(): lax.associative_scan(chain_link, (decay_re, decay_im, push_re, push_im),...  118 us
    all_gather x1, waiting for transfers between devices, body(): lax.all_gather(w_state_in, 'sp', axis=0, tiled=True)  105 us
    all_gather x1, waiting for transfers between devices, body(): lax.all_gather(w_value, 'sp', axis=0, tiled=True)  59.2 us
    all_gather x1, waiting for transfers between devices, body(): lax.all_gather(w_key, 'sp', axis=0, tiled=True)  56.1 us
    add x12, other arithmetic, chain_link(): late_are * early_bim + late_aim * early_bre + late_bim  22.2 us
    add x23, other arithmetic, local_states(): lax.associative_scan(chain_link, (decay_re, decay_im, push_re, push_im),...  21.6 us
  transfers between devices with their start and end apart: 8, of which 5 were waited for; matrix products, arithmetic and copies ran while one was open for 59% of the time, Pallas kernels for 0%

commit v1 on v0

v1 whole, which is shorter than its diff:
```python
import math

import jax
import jax.numpy as jnp
from jax import lax
from jax.experimental import pallas as pl
from jax.experimental.pallas import tpu as pltpu
from jax.sharding import PartitionSpec as P

HEAD = 64
WINDOW = 128


epsilon = 1e-06
rotary_base = 500000.0


def passed_along(value, axis, by):
    size = lax.axis_size(axis)
    pairs = [(i, i + by) for i in range(size) if 0 <= i + by < size]
    return lax.ppermute(value, axis, pairs)


def rotate(heads_block, positions):
    head_width = heads_block.shape[-1]
    half_width = head_width // 2
    frequency = rotary_base ** (-(jnp.arange(half_width, dtype=jnp.float32) * 2.0 / head_width))
    angles = positions.astype(jnp.float32)[:, None] * frequency[None, :]
    cosine = jnp.cos(angles)[:, None, :]
    sine_part = jnp.sin(angles)[:, None, :]
    lower_half = heads_block[..., :half_width]
    upper_half = heads_block[..., half_width:]
    return jnp.concatenate(
        [
            lower_half * cosine - upper_half * sine_part,
            upper_half * cosine + lower_half * sine_part,
        ],
        axis=-1,
    )


def shape_heads(query_sum, key_sum, value_sum, positions, head_width):
    row_count = query_sum.shape[0]
    kv_heads = key_sum.shape[1] // head_width
    group_size = query_sum.shape[1] // key_sum.shape[1]
    queries = rotate(
        query_sum.reshape(row_count, kv_heads * group_size, head_width), positions
    ).astype(jnp.bfloat16)
    queries = queries.reshape(row_count, kv_heads, group_size, head_width)
    key_rows = rotate(key_sum.reshape(row_count, kv_heads, head_width), positions).astype(
        jnp.bfloat16
    )
    key_rows = key_rows.reshape(row_count, kv_heads * head_width)
    value_rows = value_sum.astype(jnp.bfloat16)
    return (queries, key_rows, value_rows)


def band_attention(queries, key_rows, value_rows, sink_logit, first_row, window):
    row_count, kv_heads, group_size, head_width = queries.shape
    blocks = row_count // window
    query_blocks = queries.reshape(blocks, window, kv_heads, group_size, head_width)
    key_blocks = jnp.concatenate(
        [
            key_rows[:row_count].reshape(blocks, window, kv_heads, head_width),
            key_rows[window:].reshape(blocks, window, kv_heads, head_width),
        ],
        axis=1,
    )
    value_blocks = jnp.concatenate(
        [
            value_rows[:row_count].reshape(blocks, window, kv_heads, head_width),
            value_rows[window:].reshape(blocks, window, kv_heads, head_width),
        ],
        axis=1,
    )
    scores = jnp.einsum(
        "bqkgd,bskd->bkgqs", query_blocks, key_blocks, preferred_element_type=jnp.float32
    ) / math.sqrt(head_width)
    block_start = jnp.arange(blocks, dtype=jnp.int32)[:, None, None] * window
    query_at = first_row + block_start + jnp.arange(window, dtype=jnp.int32)[None, :, None]
    key_at = (
        first_row - window + block_start + jnp.arange(2 * window, dtype=jnp.int32)[None, None, :]
    )
    offset_gap = query_at - key_at
    visible = (offset_gap >= 0) & (offset_gap < window) & (key_at >= 0)
    scores = jnp.where(visible[:, None, None, :, :], scores, -jnp.inf)
    sink_value = sink_logit.reshape(1, kv_heads, group_size, 1, 1)
    top_score = jnp.maximum(jnp.max(scores, axis=-1, keepdims=True), sink_value)
    exponent = jnp.exp(scores - top_score)
    totals = jnp.sum(exponent, axis=-1, keepdims=True) + jnp.exp(sink_value - top_score)
    weights = (exponent / totals).astype(jnp.bfloat16)
    attended = jnp.einsum(
        "bkgqs,bskd->bqkgd", weights, value_blocks, preferred_element_type=jnp.float32
    )
    return attended.reshape(row_count, kv_heads * group_size * head_width).astype(jnp.bfloat16)


def discretize(decay_rate, rotation, log_step, in_re, in_im):
    time_step = jnp.exp(log_step)[:, None]
    lambda_re = -decay_rate
    modulus = jnp.exp(lambda_re * time_step)
    pole_re = modulus * jnp.cos(rotation * time_step)
    pole_im = modulus * jnp.sin(rotation * time_step)
    minus_one = pole_re - 1.0
    denominator = lambda_re * lambda_re + rotation * rotation
    factor_re = ((minus_one * lambda_re + pole_im * rotation) / denominator)[..., None]
    factor_im = ((pole_im * lambda_re - minus_one * rotation) / denominator)[..., None]
    drive_re = factor_re * in_re - factor_im * in_im
    drive_im = factor_re * in_im + factor_im * in_re
    return (pole_re, pole_im, drive_re, drive_im)


def split_halves(value):
    high = value.astype(jnp.bfloat16)
    low = (value - high.astype(jnp.float32)).astype(jnp.bfloat16)
    return (high, low)


def dot_f32(left, right, contract):
    return lax.dot_general(
        left, right, ((contract), ((), ())), preferred_element_type=jnp.float32
    )


def complex_mul(a_re, a_im, b_re, b_im):
    return (a_re * b_re - a_im * b_im, a_re * b_im + a_im * b_re)


def pushes(inputs, drive):
    drive_high, drive_low = split_halves(drive)
    pushed = dot_f32(inputs, drive_high, ((1,), (0,))) + dot_f32(inputs, drive_low, ((1,), (0,)))
    half = pushed.shape[1] // 2
    return (pushed[:, :half], pushed[:, half:])


def end_kernel(inputs_ref, drive_ref, pole_ref, end_ref):
    re, im = pushes(inputs_ref[...], drive_ref[0])
    rows = re.shape[0]
    powers = [(pole_ref[0, 0:1, :], pole_ref[0, 1:2, :])]
    while 2 ** len(powers) < rows:
        powers.append(complex_mul(*powers[-1], *powers[-1]))
    size = rows
    for power_re, power_im in reversed(powers):
        size = size // 2
        up_re, up_im = complex_mul(re[:size], im[:size], power_re, power_im)
        re, im = (re[size:] + up_re, im[size:] + up_im)
    end_ref[0, 0:1, :] = re
    end_ref[0, 1:2, :] = im


def shifted(value, by):
    if by % 8 == 0:
        return jnp.concatenate([jnp.zeros_like(value[:by]), value[:-by]], axis=0)
    row = lax.broadcasted_iota(jnp.int32, value.shape, 0)
    return jnp.where(row >= by, pltpu.roll(value, by, 0), 0.0)


def mix_kernel(place_ref, inputs_ref, drive_ref, pole_ref, ends_ref, out_ref, skip_ref, mixed_ref):
    inputs = inputs_ref[...]
    rows = inputs.shape[0]
    re, im = pushes(inputs, drive_ref[0])
    power_re, power_im = (pole_ref[0, 0:1, :], pole_ref[0, 1:2, :])
    far_re, far_im = (power_re, power_im)
    step = 1
    while step < rows:
        far_re, far_im = complex_mul(far_re, far_im, far_re, far_im)
        step = step * 2
    mine = place_ref[0]

    def join(position, carry):
        moved_re, moved_im = complex_mul(carry[0], carry[1], far_re, far_im)
        keep = position < mine
        piece = ends_ref[position, 0]
        return (
            jnp.where(keep, moved_re + piece[0:1], carry[0]),
            jnp.where(keep, moved_im + piece[1:2], carry[1]),
        )

    carry = (jnp.zeros_like(power_re), jnp.zeros_like(power_im))
    for position in range(ends_ref.shape[0] - 1):
        carry = join(position, carry)
    add_re, add_im = complex_mul(carry[0], carry[1], power_re, power_im)
    first = lax.broadcasted_iota(jnp.int32, re.shape, 0) == 0
    re = re + jnp.where(first, add_re, 0.0)
    im = im + jnp.where(first, add_im, 0.0)
    step = 1
    while step < rows:
        move_re, move_im = complex_mul(shifted(re, step), shifted(im, step), power_re, power_im)
        re, im = (re + move_re, im + move_im)
        power_re, power_im = complex_mul(power_re, power_im, power_re, power_im)
        step = step * 2
    state_high, state_low = split_halves(jnp.concatenate([re, im], axis=1))
    out_high, out_low = split_halves(out_ref[0])
    contract = ((1,), (1,))
    summed = (
        dot_f32(state_high, out_high, contract)
        + dot_f32(state_low, out_high, contract)
        + dot_f32(state_high, out_low, contract)
    )
    summed = summed + skip_ref[0] * inputs.astype(jnp.float32)
    mixed_ref[...] = jax.nn.gelu(summed).astype(jnp.bfloat16)


def spread(compact, per_block):
    groups, width, states = compact.shape
    tiled = jnp.tile(
        compact.reshape(groups // per_block, per_block * width, states), (1, 1, per_block)
    )
    row_group = lax.broadcasted_iota(jnp.int32, tiled.shape, 1) // width
    lane_group = lax.broadcasted_iota(jnp.int32, tiled.shape, 2) // states
    return jnp.where(row_group == lane_group, tiled, 0.0)


def state_params(decay_rate, rotation, log_step, in_re, in_im, out_re, out_im):
    groups, states, group_width = in_re.shape
    per_block = math.gcd(groups, 128 // group_width)
    blocks = groups // per_block
    pole_re, pole_im, drive_re, drive_im = discretize(decay_rate, rotation, log_step, in_re, in_im)
    drive = jnp.concatenate(
        [
            spread(jnp.swapaxes(drive_re, 1, 2), per_block),
            spread(jnp.swapaxes(drive_im, 1, 2), per_block),
        ],
        axis=2,
    )
    readout = jnp.concatenate([spread(out_re, per_block), spread(-out_im, per_block)], axis=2)
    poles = jnp.stack(
        [pole_re.reshape(blocks, per_block * states), pole_im.reshape(blocks, per_block * states)],
        axis=1,
    )
    return (poles, drive, readout)


def state_ends(inputs, poles, drive):
    blocks, channels, wide = drive.shape
    rows = inputs.shape[0]
    return pl.pallas_call(
        end_kernel,
        grid=(blocks,),
        in_specs=[
            pl.BlockSpec((rows, channels), lambda b: (0, b)),
            pl.BlockSpec((1, channels, wide), lambda b: (b, 0, 0)),
            pl.BlockSpec((1, 2, wide // 2), lambda b: (b, 0, 0)),
        ],
        out_specs=pl.BlockSpec((1, 2, wide // 2), lambda b: (b, 0, 0)),
        out_shape=jax.ShapeDtypeStruct((blocks, 2, wide // 2), jnp.float32),
    )(inputs, drive, poles)


def state_mix(inputs, poles, drive, readout, ends, skip_gain):
    blocks, channels, wide = drive.shape
    rows = inputs.shape[0]
    place = lax.axis_index("sp").astype(jnp.int32).reshape(1)
    return pl.pallas_call(
        mix_kernel,
        grid=(blocks,),
        in_specs=[
            pl.BlockSpec(memory_space=pltpu.SMEM),
            pl.BlockSpec((rows, channels), lambda b: (0, b)),
            pl.BlockSpec((1, channels, wide), lambda b: (b, 0, 0)),
            pl.BlockSpec((1, 2, wide // 2), lambda b: (b, 0, 0)),
            pl.BlockSpec((ends.shape[0], 1, 2, wide // 2), lambda b: (0, b, 0, 0)),
            pl.BlockSpec((1, channels, wide), lambda b: (b, 0, 0)),
            pl.BlockSpec((1, 1, channels), lambda b: (b, 0, 0)),
        ],
        out_specs=pl.BlockSpec((rows, channels), lambda b: (0, b)),
        out_shape=jax.ShapeDtypeStruct(inputs.shape, jnp.bfloat16),
    )(place, inputs, drive, poles, ends, readout, skip_gain.reshape(blocks, 1, channels))


def flow_kernel(inputs_ref, drive_ref, pole_ref, out_ref, skip_ref, mixed_ref, carry_ref):
    @pl.when(pl.program_id(0) == 0)
    def _():
        carry_ref[...] = jnp.zeros_like(carry_ref)

    inputs = inputs_ref[...]
    rows = inputs.shape[0]
    re, im = pushes(inputs, drive_ref[0])
    power_re, power_im = (pole_ref[0, 0:1, :], pole_ref[0, 1:2, :])
    add_re, add_im = complex_mul(carry_ref[0:1, :], carry_ref[1:2, :], power_re, power_im)
    first = lax.broadcasted_iota(jnp.int32, re.shape, 0) == 0
    re = re + jnp.where(first, add_re, 0.0)
    im = im + jnp.where(first, add_im, 0.0)
    step = 1
    while step < rows:
        move_re, move_im = complex_mul(shifted(re, step), shifted(im, step), power_re, power_im)
        re, im = (re + move_re, im + move_im)
        power_re, power_im = complex_mul(power_re, power_im, power_re, power_im)
        step = step * 2
    carry_ref[0:1, :] = re[rows - 1 :]
    carry_ref[1:2, :] = im[rows - 1 :]
    state_high, state_low = split_halves(jnp.concatenate([re, im], axis=1))
    out_high, out_low = split_halves(out_ref[0])
    contract = ((1,), (1,))
    summed = (
        dot_f32(state_high, out_high, contract)
        + dot_f32(state_low, out_high, contract)
        + dot_f32(state_high, out_low, contract)
    )
    summed = summed + skip_ref[...] * inputs.astype(jnp.float32)
    mixed_ref[...] = jax.nn.gelu(summed).astype(jnp.bfloat16)


def state_flow(inputs, poles, drive, readout, skip_gain, chunk):
    _, channels, wide = drive.shape
    rows = inputs.shape[0]
    return pl.pallas_call(
        flow_kernel,
        grid=(rows // chunk,),
        in_specs=[
            pl.BlockSpec((chunk, channels), lambda t: (t, 0)),
            pl.BlockSpec((1, channels, wide), lambda t: (0, 0, 0)),
            pl.BlockSpec((1, 2, wide // 2), lambda t: (0, 0, 0)),
            pl.BlockSpec((1, channels, wide), lambda t: (0, 0, 0)),
            pl.BlockSpec((1, channels), lambda t: (0, 0)),
        ],
        out_specs=pl.BlockSpec((chunk, channels), lambda t: (t, 0)),
        out_shape=jax.ShapeDtypeStruct(inputs.shape, jnp.bfloat16),
        scratch_shapes=[pltpu.VMEM((2, wide // 2), jnp.float32)],
    )(inputs, drive, poles, readout, skip_gain.reshape(1, channels))


def out_kernel(acts_ref, w_ref, sum_ref):
    cores = w_ref.shape[0]
    total = None
    for core in range(cores):
        rows = jnp.concatenate(
            [acts_ref[at] for at in range(core, acts_ref.shape[0], cores)], axis=1
        )
        piece = dot_f32(rows, w_ref[core], ((1,), (0,)))
        piece = piece.astype(jnp.bfloat16).astype(jnp.float32)
        total = piece if total is None else total + piece
    sum_ref[...] = total.astype(jnp.bfloat16)


def out_project(acts, w_pair):
    devices, rows, width = acts.shape
    cores, depth, columns = w_pair.shape
    block = math.gcd(rows, 256)
    return pl.pallas_call(
        out_kernel,
        grid=(rows // block,),
        in_specs=[
            pl.BlockSpec((devices, block, width), lambda t: (0, t, 0)),
            pl.BlockSpec((cores, depth, columns), lambda t: (0, 0, 0)),
        ],
        out_specs=pl.BlockSpec((block, columns), lambda t: (t, 0)),
        out_shape=jax.ShapeDtypeStruct((rows, columns), jnp.bfloat16),
    )(acts, w_pair)


def own_part(value, axis_name):
    size = value.shape[0] // lax.axis_size(axis_name)
    return lax.dynamic_slice_in_dim(value, lax.axis_index(axis_name) * size, size, 0)


def normalize(tokens, norm_gain):
    wide_tokens = tokens.astype(jnp.float32)
    return (
        wide_tokens
        * lax.rsqrt(jnp.mean(wide_tokens * wide_tokens, axis=-1, keepdims=True) + epsilon)
        * norm_gain
    ).astype(jnp.bfloat16)


def by_heads(
    tokens,
    norm_gain,
    w_query,
    w_key,
    w_value,
    w_state_in,
    sink_logit,
    decay_rate,
    rotation,
    log_step,
    in_re,
    in_im,
    out_re,
    out_im,
    skip_gain,
    w_attn_out,
    w_state_out,
    out_gain,
):
    devices = lax.axis_size("sp")
    row_count = tokens.shape[0]
    everyone = ("sp", "tp")
    normed = lax.all_gather(
        normalize(own_part(tokens, "tp"), norm_gain), everyone, axis=0, tiled=True
    )
    rows = normed.shape[0]
    depth = w_query.shape[0]
    repeats = devices // (w_key.shape[1] // HEAD)

    def per_device(weight):
        return weight.reshape(depth, devices, weight.shape[1] // devices)

    def per_head(weight):
        return jnp.repeat(weight.reshape(depth, -1, HEAD), repeats, axis=1)

    pieces = (per_device(w_query), per_head(w_key), per_head(w_value), per_device(w_state_in))
    key_at = pieces[0].shape[2]
    value_at = key_at + HEAD
    input_at = value_at + HEAD
    parcels = jnp.concatenate(pieces, axis=2).transpose(1, 0, 2)
    w_in = lax.all_to_all(parcels, "sp", split_axis=0, concat_axis=0, tiled=True)
    w_in = w_in.reshape(devices * depth, parcels.shape[2])

    def rows_of(weight):
        return weight.reshape(devices, weight.shape[0] // devices, weight.shape[1])

    w_out = jnp.concatenate([rows_of(w_attn_out), rows_of(w_state_out)], axis=1)
    w_out = w_out.reshape(1, -1, w_out.shape[2])
    w_pair = lax.all_to_all(w_out, "tp", split_axis=2, concat_axis=0, tiled=True)
    decay_rate, rotation, log_step, in_re, in_im, out_re, out_im, skip_gain, sink_logit = [
        own_part(value, "sp")
        for value in (
            decay_rate, rotation, log_step, in_re, in_im, out_re, out_im, skip_gain, sink_logit
        )
    ]
    poles, drive, readout = state_params(
        decay_rate, rotation, log_step, in_re, in_im, out_re, out_im
    )
    sums = jnp.dot(normed, w_in, preferred_element_type=jnp.float32)
    inputs = sums[:, input_at:].astype(jnp.bfloat16)
    queries, key_rows, value_rows = shape_heads(
        sums[:, :key_at],
        sums[:, key_at:value_at],
        sums[:, value_at:input_at],
        jnp.arange(rows, dtype=jnp.int32),
        HEAD,
    )

    def padded(value):
        return jnp.pad(value, ((WINDOW, 0), (0, 0))).reshape(WINDOW + rows, 1, HEAD)

    attended = band_attention(
        queries, padded(key_rows), padded(value_rows), sink_logit, jnp.int32(0), WINDOW
    )
    mixed_state = state_flow(inputs, poles, drive, readout, skip_gain, row_count)
    acts = lax.all_gather(
        jnp.concatenate([attended, mixed_state], axis=1), everyone, axis=0, tiled=False
    )
    summed = out_project(acts, w_pair)
    projected = lax.all_to_all(summed, everyone, split_axis=0, concat_axis=1, tiled=True)
    projected = projected.astype(jnp.float32)
    row_scale = lax.rsqrt(jnp.mean(projected * projected, axis=-1, keepdims=True) + epsilon)
    return (projected * row_scale * out_gain).astype(jnp.bfloat16)


def everyones(value, axis):
    size = lax.axis_size(axis)
    copies = jnp.broadcast_to(value[None], (size,) + value.shape)
    return lax.all_to_all(copies, axis, split_axis=0, concat_axis=0, tiled=True)


def earlier_window(key_rows, value_rows):
    joined = jnp.concatenate([key_rows, value_rows], axis=1)
    prior = passed_along(joined, "sp", 1)
    return jnp.concatenate([prior, joined], axis=0)


def by_tokens(
    tokens,
    norm_gain,
    w_query,
    w_key,
    w_value,
    w_state_in,
    sink_logit,
    decay_rate,
    rotation,
    log_step,
    in_re,
    in_im,
    out_re,
    out_im,
    skip_gain,
    w_attn_out,
    w_state_out,
    out_gain,
):
    row_count = tokens.shape[0]
    window = WINDOW
    head_width = HEAD
    wide_tokens = tokens.astype(jnp.float32)
    normed = (
        wide_tokens
        * lax.rsqrt(jnp.mean(wide_tokens * wide_tokens, axis=-1, keepdims=True) + epsilon)
        * norm_gain
    ).astype(jnp.bfloat16)
    first_row = lax.axis_index("sp") * row_count
    positions = first_row + jnp.arange(row_count, dtype=jnp.int32)
    poles, drive, readout = state_params(
        decay_rate, rotation, log_step, in_re, in_im, out_re, out_im
    )
    slab = lax.all_to_all(normed, "sp", split_axis=1, concat_axis=0, tiled=True)
    w_in = jnp.concatenate([w_query, w_key, w_value, w_state_in], axis=1)
    sums = lax.psum_scatter(
        jnp.dot(slab, w_in, preferred_element_type=jnp.float32).astype(jnp.bfloat16),
        "sp",
        scatter_dimension=0,
        tiled=True,
    )
    key_at = w_query.shape[1]
    value_at = key_at + w_key.shape[1]
    input_at = value_at + w_value.shape[1]
    inputs = sums[:, input_at:]
    ends = everyones(state_ends(inputs, poles, drive), "sp")
    queries, key_rows, value_rows = shape_heads(
        sums[:, :key_at].astype(jnp.float32),
        sums[:, key_at:value_at].astype(jnp.float32),
        sums[:, value_at:input_at],
        positions,
        head_width,
    )
    joined_rows = earlier_window(key_rows, value_rows)
    kv_width = key_rows.shape[1]
    kv_heads = kv_width // head_width
    all_keys = joined_rows[:, :kv_width].reshape(window + row_count, kv_heads, head_width)
    all_values = joined_rows[:, kv_width:].reshape(window + row_count, kv_heads, head_width)
    attended = band_attention(queries, all_keys, all_values, sink_logit, first_row, window)
    mixed_state = state_mix(inputs, poles, drive, readout, ends, skip_gain)
    rows = lax.all_gather(
        jnp.concatenate([attended, mixed_state], axis=1), "sp", axis=0, tiled=True
    )
    w_out = jnp.concatenate([w_attn_out, w_state_out], axis=0)
    partial = jnp.dot(rows, w_out, preferred_element_type=jnp.float32).astype(jnp.bfloat16)
    cores = lax.axis_size("tp")
    blocks = partial.reshape(-1, cores, row_count // cores, partial.shape[1])
    halves = lax.all_to_all(blocks, "tp", split_axis=1, concat_axis=1, tiled=True)
    summed = jnp.sum(halves.astype(jnp.float32), axis=1).astype(jnp.bfloat16)
    projected = lax.all_to_all(summed, "sp", split_axis=0, concat_axis=2, tiled=True)
    projected = projected.reshape(row_count // cores, -1).astype(jnp.float32)
    row_scale = lax.rsqrt(jnp.mean(projected * projected, axis=-1, keepdims=True) + epsilon)
    return (projected * row_scale * out_gain).astype(jnp.bfloat16)


def body(tokens, norm_gain, w_query, w_key, *others):
    devices = lax.axis_size("sp")
    heads = w_query.shape[1] // HEAD
    groups = others[5].shape[0]
    group_size = w_query.shape[1] // w_key.shape[1]
    fits = (
        heads % devices == 0
        and groups % devices == 0
        and group_size % max(heads // devices, 1) == 0
        and tokens.shape[0] % (8 * lax.axis_size("tp")) == 0
    )
    return (by_heads if fits else by_tokens)(tokens, norm_gain, w_query, w_key, *others)


def solution(mesh):
    return jax.shard_map(
        body,
        mesh=mesh,
        in_specs=(
            P("sp", None),
            P(),
            P("sp", "tp"),
            P("sp", "tp"),
            P("sp", "tp"),
            P("sp", "tp"),
            P("tp"),
            P("tp", None),
            P("tp", None),
            P("tp"),
            P("tp", None, None),
            P("tp", None, None),
            P("tp", None, None),
            P("tp", None, None),
            P("tp"),
            P("tp", "sp"),
            P("tp", "sp"),
            P(),
        ),
        out_specs=P(("sp", "tp"), None),
        check_vma=False,
    )
```

time: 1020 us -> 352 us (0.35); the launches traced: 1010 us -> 350 us
  local copies, waits for them, and re-layouts: 469 us -> 16.4 us
  blocking collectives: 152 us -> 23 us
  other arithmetic: 96.5 us -> 24.6 us
  matrix products: 40 us -> 13.4 us
  Pallas kernels: 0 us -> 25.1 us
    slice x48 -> x1, local copies, waits for them, and re-layouts: 307 us -> 1.04 us  [by_heads(): sums[:, value_at:input_at]]
    all_gather x4 -> x0, blocking collectives: 152 us -> none  [carried_in(): pieces = jax.tree.map(lambda part: lax.all_gather(part, axis), value)]
    pad x48 -> x0, local copies, waits for them, and re-layouts: 118 us -> none  [local_states(): lax.associative_scan(chain_link, (decay_re, decay_im, push_re, push_im),...]
    add x45 -> x1, other arithmetic: 64.2 us -> 0.07 us  [band_attention(): first_row + block_start + jnp.arange(window, dtype=jnp.int32)[None, :, None]]
    all_to_all x0 -> x1, waiting for transfers between devices: none -> 57.7 us  [by_heads(): lax.all_to_all(parcels, 'sp', split_axis=0, concat_axis=0, tiled=True)]
    all_gather x6 -> x2, waiting for transfers between devices: 220 us -> 168 us  [the longest x1 94.8 us: by_heads(): lax.all_gather(jnp.concatenate([attended, mixed_state], axis=1), everyone...]
    dot_general x10 -> x1, matrix products: 38.3 us -> 8.75 us  [by_heads(): sums = jnp.dot(normed, w_in, preferred_element_type=jnp.float32)]
    pallas_call x0 -> x2, Pallas kernels: none -> 25.1 us  [the longest x1 13.6 us: state_flow(): pl.pallas_call(flow_kernel, grid=(rows // chunk,), in_specs=[pl.BlockSpec...]
  transfers between devices with their start and end apart: 8 -> 3, of which waited for: 5 -> 3; matrix products, arithmetic and copies ran while one was open for 59% -> 7% of each run, Pallas kernels for 0% -> 0%
where the time goes in v1:
time: 352 us; the launch traced here: 350 us
  waiting for transfers between devices  225 us (64%)
  Pallas kernels  25.1 us (7%)
  other arithmetic  24.6 us (7%)
  blocking collectives  23 us (7%)
  local copies, waits for them, and re-layouts  16.4 us (5%)
  between operations  13.8 us (4%)
  matrix products  13.4 us (4%)
  starting transfers between devices  8.55 us (2%)
    all_gather x1, waiting for transfers between devices, by_heads(): lax.all_gather(jnp.concatenate([attended, mixed_state], axis=1), everyone...  94.8 us
    all_gather x1, waiting for transfers between devices, by_heads(): lax.all_gather(normalize(own_part(tokens, 'tp'), norm_gain), everyone, ax...  72.9 us
    all_to_all x1, waiting for transfers between devices, by_heads(): lax.all_to_all(parcels, 'sp', split_axis=0, concat_axis=0, tiled=True)  57.7 us
    all_to_all x1, blocking collectives, by_heads(): lax.all_to_all(summed, everyone, split_axis=0, concat_axis=1, tiled=True)  18.4 us
    pallas_call x1, Pallas kernels, state_flow(): pl.pallas_call(flow_kernel, grid=(rows // chunk,), in_specs=[pl.BlockSpec...  13.6 us
    pallas_call x1, Pallas kernels, out_project(): pl.pallas_call(out_kernel, grid=(rows // block,), in_specs=[pl.BlockSpec(...  11.4 us
    unnamed x3, other arithmetic  9.21 us
    dot_general x1, matrix products, by_heads(): sums = jnp.dot(normed, w_in, preferred_element_type=jnp.float32)  8.75 us
  transfers between devices with their start and end apart: 3, of which 3 were waited for; matrix products, arithmetic and copies ran while one was open for 7% of the time, Pallas kernels for 0%

profile of v1, /device:TPU:0, one launch (start us, length us, event | category | flops | bytes accessed | tf_op | source)
XLA Modules:
  0.0 350.3 jit_solution(11413336124778774696)
XLA Ops:
  6.6 1.3 fusion.4
  8.0 2.0 fusion.6
  10.8 1.5 maximum_bitcast_fusion
  12.3 8.5 %all-to-all-start = ((bf16[16,256,256]{1,2,0:T(8,128)(2,1)}), bf16[16,256,256]{1,2,0:T(8,128)(2,1)S(1)}, u32[]{:S(2)}, u32[]{:S(2)}) async-start(bf16[16,256,256]{1,2,0:T(8,128)(2,1)} %maximum_bitcast_fusion), calls=%async_computation | async-start | bytes 4194304 | tf_op jit(solution)/shard_map/all_to_all | solution.py:407
  21.0 0.8 add_divide_fusion
  22.0 0.7 subtract_divide_fusion
  22.7 0.8 multiply_subtract_fusion
  23.8 0.8 dynamic-slice_negate_fusion
  27.6 0.7 pad_maximum_fusion.3.out_ref
  28.5 57.7 %all-to-all-done = bf16[16,256,256]{1,2,0:T(8,128)(2,1)S(1)} async-done(((bf16[16,256,256]{1,2,0:T(8,128)(2,1)}), bf16[16,256,256]{1,2,0:T(8,128)(2,1)S(1)}, u32[]{:S(2)}, u32[]{:S(2)}) %all-to-all-start) | async-done | bytes 2097184 | tf_op jit(solution)/shard_map/all_to_all | solution.py:407
  86.2 2.4 copy.72
  88.6 72.9 %all-gather.4.cloned.1.call-done = bf16[2048,4096]{1,0:T(8,128)(2,1)} async-done(((bf16[64,4096]{1,0:T(8,128)(2,1)}), bf16[2048,4096]{1,0:T(8,128)(2,1)}) %all-gather.4.cloned.1.call-update) | async-done | bytes 16777232 | tf_op jit(solution)/shard_map/all_gather | solution.py:389
  161.5 8.8 %fusion.47 = f32[2048,256]{0,1:T(8,128)S(1)} fusion(bf16[2048,4096]{1,0:T(8,128)(2,1)} %all-gather.4.cloned.1.call-done, bf16[4096,256]{1,0:T(8,128)(2,1)} %bitcast.108), kind=kOutput, calls=%fused_computation.114 | convolution fusion | flops 4294967296 | bytes 20971520 | tf_op jit(solution)/shard_map/dot_general | solution.py:425
  170.3 1.0 slice_bitcast_fusion
  171.9 2.3 fusion.41
  174.6 4.1 %fusion.46 = (f32[16,128]{1,0:T(8,128)S(1)}, f32[16,1,1,128,256]{3,4,0,2,1:T(8,128)S(1)}) fusion(bf16[16,128,32]{1,2,0:T(8,128)(2,1)S(1)} %copy.80, bf16[16,128,32]{1,2,0:T(8,128)(2,1)S(1)} %copy.79, bf16[16,128,1,32]{1,3,0,2:T(8,128)(2,1)S(1)} %get-tuple-element.32, bf16[16,128,1,32]{1,3,0,2:T(8,128)(2,1)S(1)} %get-tuple-element.33, ...), kind=kOutput, calls=%fused_computation.113 | convolution fusion | flops 73398272 | bytes 2920448 | tf_op jit(solution)/shard_map/bqkgd,bskd->bkgqs/dot_general | solution.py:76
  178.7 0.7 broadcast_maximum_fusion
  179.7 0.7 exponential_add_fusion
  180.4 1.0 fusion.45
  182.0 1.0 copy-done.3
  183.9 13.6 %shard_map.172 = bf16[2048,64]{1,0:T(8,128)(2,1)} custom-call(bf16[2048,64]{1,0:T(8,128)(2,1)} %get-tuple-element.13.inputs_ref, f32[1,64,512]{2,1,0:T(8,128)} %pad_maximum_fusion.2.drive_ref, f32[1,2,256]{2,1,0:T(2,128)} %pad_maximum_fusion.4.pole_ref, f32[1,64,512]{2,1,0:T(8,128)} %pad_maximum_fusion.3.out_ref, f32[1,64]{1,0:T(1,128)} %dynamic-slice_bitcast_fusion.skip_ref), custom_call_target="tpu_custom_call" | custom-call | tf_op jit(solution)/shard_map/pallas_call | solution.py:307
  197.6 2.1 pad_maximum_fusion.1
  199.8 2.2 copy.83
  202.6 6.8 %reduce.4 = bf16[256,2048]{1,0:T(8,128)(2,1)S(1)} reduce(bf16[256,1,2048]{2,1,0:T(2,128)(2,1)S(1)} %bitcast.101, bf16[]{:T(256)} %broadcast.820), dimensions={1}, to_apply=%bitcast.88.reduce_sub_computation | reduce | bytes 2097154
  209.4 0.8 reshape.941
  210.2 4.6 %all_to_all.36 = bf16[2,2,131072]{2,1,0:T(2,128)(2,1)S(1)} all-to-all(bf16[2,2,131072]{2,1,0:T(2,128)(2,1)S(1)} %reshape.941), channel_id=1, replica_groups=mesh['sp'=16,'tp'=2] {'tp'}, dimensions={0} | all-to-all | bytes 2097152 | tf_op jit(solution)/shard_map/all_to_all | solution.py:415
  214.8 0.9 reshape.942
  216.3 1.3 copy.84
  217.7 94.8 %all-gather.6.cloned.1.call-done = bf16[65536,128]{1,0:T(8,128)(2,1)} async-done(((bf16[2048,128]{1,0:T(8,128)(2,1)}), bf16[65536,128]{1,0:T(8,128)(2,1)}) %all-gather.6.cloned.1.call-update) | async-done | bytes 16777232 | tf_op jit(solution)/shard_map/all_gather | solution.py:442
  312.4 11.4 %shard_map.173 = bf16[2048,128]{1,0:T(8,128)(2,1)} custom-call(bf16[32,2048,128]{2,1,0:T(8,128)(2,1)} %bitcast.99, bf16[2,2048,128]{2,1,0:T(8,128)(2,1)} %bitcast.103), custom_call_target="tpu_custom_call" | custom-call | tf_op jit(solution)/shard_map/pallas_call | solution.py:340
  323.8 18.4 %all_to_all.37 = bf16[32,64,128]{2,1,0:T(8,128)(2,1)S(1)} all-to-all(bf16[32,64,128]{2,1,0:T(8,128)(2,1)} %bitcast.107), channel_id=1, replica_groups=mesh['sp'=16,'tp'=2] {'sp','tp'}, dimensions={0} | all-to-all | bytes 1048576 | tf_op jit(solution)/shard_map/all_to_all | solution.py:446
  342.5 1.0 fusion.9
  (83 shorter events, 8.7 us)
Async XLA Ops:
  6.5 19.1 %copy-start = (f32[1024]{0:T(1024)S(1)}, f32[1024]{0:T(1024)}, u32[]{:S(2)}) copy-start(f32[1024]{0:T(1024)} %param.32) | copy-start | bytes 12292
  6.5 3.5 copy-start.8
  6.5 3.6 %copy-start.9 = (bf16[256,256]{1,0:T(8,128)(2,1)S(1)}, bf16[256,256]{1,0:T(8,128)(2,1)}, u32[]{:S(2)}) copy-start(bf16[256,256]{1,0:T(8,128)(2,1)} %param.22) | copy-start | bytes 393220
  6.5 3.7 %copy-start.4 = (bf16[256,1024]{1,0:T(8,128)(2,1)S(1)}, bf16[256,1024]{1,0:T(8,128)(2,1)}, u32[]{:S(2)}) copy-start(bf16[256,1024]{1,0:T(8,128)(2,1)} %param.20) | copy-start | bytes 1572868
  6.5 3.9 %copy-start.5 = (bf16[256,1024]{1,0:T(8,128)(2,1)S(1)}, bf16[256,1024]{1,0:T(8,128)(2,1)}, u32[]{:S(2)}) copy-start(bf16[256,1024]{1,0:T(8,128)(2,1)} %param.23) | copy-start | bytes 1572868
  6.5 155.0 %all-gather.4.cloned.1.call-start = ((), (), s32[]{:S(2)}) async-start(), calls=%async_computation.3 | async-start | bytes 17301504 | tf_op jit(solution)/shard_map/all_gather | solution.py:389
  12.3 8.5 %copy-start.11 = (f32[64]{0:T(128)S(1)}, f32[64]{0:T(128)}, u32[]{:S(2)}) copy-start(f32[64]{0:T(128)} %param.27) | copy-start | bytes 772
  12.3 12.6 %copy-start.12 = (f32[16]{0:T(128)S(1)}, f32[16]{0:T(128)}, u32[]{:S(2)}) copy-start(f32[16]{0:T(128)} %param.24) | copy-start | bytes 196
  12.3 73.9 %all-to-all-start = ((bf16[16,256,256]{1,2,0:T(8,128)(2,1)}), bf16[16,256,256]{1,2,0:T(8,128)(2,1)S(1)}, u32[]{:S(2)}, u32[]{:S(2)}) async-start(bf16[16,256,256]{1,2,0:T(8,128)(2,1)} %maximum_bitcast_fusion), calls=%async_computation | async-start | bytes 4194304 | tf_op jit(solution)/shard_map/all_to_all | solution.py:407
  20.8 291.6 %all-gather.6.cloned.1.call-start = ((), (), s32[]{:S(2)}) async-start(), calls=%async_computation.4 | async-start | bytes 17301504 | tf_op jit(solution)/shard_map/all_gather | solution.py:442
  178.7 2.8 copy-start.2
  181.5 1.6 copy-start.3
  183.6 16.1 %copy-start.6 = (bf16[1024,256]{1,0:T(8,128)(2,1)S(1)}, bf16[1024,256]{1,0:T(8,128)(2,1)}, u32[]{:S(2)}) copy-start(bf16[1024,256]{1,0:T(8,128)(2,1)} %param.34) | copy-start | bytes 1572868
  183.6 16.1 %copy-start.7 = (bf16[1024,256]{1,0:T(8,128)(2,1)S(1)}, bf16[1024,256]{1,0:T(8,128)(2,1)}, u32[]{:S(2)}) copy-start(bf16[1024,256]{1,0:T(8,128)(2,1)} %param.33) | copy-start | bytes 1572868
  312.4 30.1 %copy-start.10 = (f32[4096]{0:T(1024)S(1)}, f32[4096]{0:T(1024)}, u32[]{:S(2)}) copy-start(f32[4096]{0:T(1024)} %param.35) | copy-start | bytes 49156
  312.4 31.1 %copy-start.1 = (f32[1024]{0:T(1024)S(1)}, f32[1024]{0:T(1024)}, u32[]{:S(2)}) copy-start(f32[1024]{0:T(1024)} %param.32) | copy-start | bytes 12292
Sparse Core Ops, SparseCore 0:
  10.2 151.2 all-gather.3
  199.8 112.5 all-gather.5

commit v2 on v1

--- a/solution.py
+++ b/solution.py
@@ -268,56 +268,134 @@
     )(place, inputs, drive, poles, ends, readout, skip_gain.reshape(blocks, 1, channels))
 
 
-def flow_kernel(inputs_ref, drive_ref, pole_ref, out_ref, skip_ref, mixed_ref, carry_ref):
-    @pl.when(pl.program_id(0) == 0)
+def attend(queries, keys, values, old_keys, old_values, sink, first):
+    rows = queries.shape[0]
+    contract = ((1,), (1,))
+    scale = 1.0 / math.sqrt(HEAD)
+    row = lax.broadcasted_iota(jnp.int32, (rows, rows), 0)
+    column = lax.broadcasted_iota(jnp.int32, (rows, rows), 1)
+    old_seen = column > row if first is None else (column > row) & jnp.logical_not(first)
+    old = jnp.where(old_seen, dot_f32(queries, old_keys, contract) * scale, -jnp.inf)
+    new = jnp.where(column <= row, dot_f32(queries, keys, contract) * scale, -jnp.inf)
+    top = jnp.max(jnp.maximum(old, new), axis=-1, keepdims=True)
+    top = jnp.maximum(top, sink)
+    old = jnp.exp(old - top)
+    new = jnp.exp(new - top)
+    totals = jnp.sum(old + new, axis=-1, keepdims=True) + jnp.exp(sink - top)
+    plain = ((1,), (0,))
+    return dot_f32((old / totals).astype(jnp.bfloat16), old_values, plain) + dot_f32(
+        (new / totals).astype(jnp.bfloat16), values, plain
+    )
+
+
+def layer_kernel(
+    sink_ref, normed_ref, w_ref, cosine_ref, sine_ref, drive_ref, pole_ref, out_ref, skip_ref,
+    acts_ref, keys_ref, values_ref, carry_ref,
+):
+    start = pl.program_id(0) == 0
+
+    @pl.when(start)
     def _():
         carry_ref[...] = jnp.zeros_like(carry_ref)
-
-    inputs = inputs_ref[...]
-    rows = inputs.shape[0]
-    re, im = pushes(inputs, drive_ref[0])
-    power_re, power_im = (pole_ref[0, 0:1, :], pole_ref[0, 1:2, :])
-    add_re, add_im = complex_mul(carry_ref[0:1, :], carry_ref[1:2, :], power_re, power_im)
-    first = lax.broadcasted_iota(jnp.int32, re.shape, 0) == 0
-    re = re + jnp.where(first, add_re, 0.0)
-    im = im + jnp.where(first, add_im, 0.0)
-    step = 1
-    while step < rows:
-        move_re, move_im = complex_mul(shifted(re, step), shifted(im, step), power_re, power_im)
-        re, im = (re + move_re, im + move_im)
-        power_re, power_im = complex_mul(power_re, power_im, power_re, power_im)
-        step = step * 2
-    carry_ref[0:1, :] = re[rows - 1 :]
-    carry_ref[1:2, :] = im[rows - 1 :]
-    state_high, state_low = split_halves(jnp.concatenate([re, im], axis=1))
-    out_high, out_low = split_halves(out_ref[0])
-    contract = ((1,), (1,))
-    summed = (
-        dot_f32(state_high, out_high, contract)
-        + dot_f32(state_low, out_high, contract)
-        + dot_f32(state_high, out_low, contract)
-    )
-    summed = summed + skip_ref[...] * inputs.astype(jnp.float32)
-    mixed_ref[...] = jax.nn.gelu(summed).astype(jnp.bfloat16)
-
-
-def state_flow(inputs, poles, drive, readout, skip_gain, chunk):
-    _, channels, wide = drive.shape
-    rows = inputs.shape[0]
+        keys_ref[...] = jnp.zeros_like(keys_ref)
+        values_ref[...] = jnp.zeros_like(values_ref)
+
+    sums = dot_f32(normed_ref[...], w_ref[...], ((1,), (0,)))
+    chunk = WINDOW
+    wide = 2 * HEAD
+    lane = lax.broadcasted_iota(jnp.int32, (chunk, wide), 1)
+    sink = sink_ref[0]
+    drive_high, drive_low = split_halves(drive_ref[...])
+    out_high, out_low = split_halves(out_ref[...])
+    powers = [(pole_ref[0, 0:1, :], pole_ref[0, 1:2, :])]
+    while 2 ** len(powers) < chunk:
+        powers.append(complex_mul(*powers[-1], *powers[-1]))
+    old_keys, old_values = (keys_ref[...], values_ref[...])
+    carry_re, carry_im = (carry_ref[0:1, :], carry_ref[1:2, :])
+    for at in range(0, sums.shape[0], chunk):
+        turned = sums[at : at + chunk, :wide]
+        swapped = jnp.where(
+            lane % HEAD < HEAD // 2,
+            pltpu.roll(turned, wide - HEAD // 2, 1),
+            pltpu.roll(turned, HEAD // 2, 1),
+        )
+        turned = turned * cosine_ref[at : at + chunk] + swapped * sine_ref[at : at + chunk]
+        queries = jnp.where(lane < HEAD, turned, 0.0).astype(jnp.bfloat16)
+        keys = pltpu.roll(turned, HEAD, 1).astype(jnp.bfloat16)
+        values = sums[at : at + chunk, wide:].astype(jnp.bfloat16)
+        attended = attend(
+            queries, keys, values, old_keys, old_values, sink, start if at == 0 else None
+        )
+        old_keys, old_values = (keys, values)
+        plain = ((1,), (0,))
+        pushed = dot_f32(values, drive_high, plain) + dot_f32(values, drive_low, plain)
+        half = pushed.shape[1] // 2
+        re, im = (pushed[:, :half], pushed[:, half:])
+        add_re, add_im = complex_mul(carry_re, carry_im, *powers[0])
+        first = lax.broadcasted_iota(jnp.int32, re.shape, 0) == 0
+        re = re + jnp.where(first, add_re, 0.0)
+        im = im + jnp.where(first, add_im, 0.0)
+        for level, power in enumerate(powers):
+            move_re, move_im = complex_mul(
+                shifted(re, 2**level), shifted(im, 2**level), *power
+            )
+            re, im = (re + move_re, im + move_im)
+        carry_re, carry_im = (re[chunk - 1 :], im[chunk - 1 :])
+        state_high, state_low = split_halves(jnp.concatenate([re, im], axis=1))
+        contract = ((1,), (1,))
+        summed = (
+            dot_f32(state_high, out_high, contract)
+            + dot_f32(state_low, out_high, contract)
+            + dot_f32(state_high, out_low, contract)
+        )
+        mixed = jax.nn.gelu(summed + skip_ref[...] * values.astype(jnp.float32))
+        acts_ref[at : at + chunk, :] = jnp.where(lane < HEAD, attended, mixed).astype(
+            jnp.bfloat16
+        )
+    keys_ref[...] = old_keys
+    values_ref[...] = old_values
+    carry_ref[0:1, :] = carry_re
+    carry_ref[1:2, :] = carry_im
+
+
+def layer(normed, w_in, cosine, sine, sink_logit, poles, drive, readout, skip_gain):
+    rows, depth = normed.shape
+    block = math.gcd(rows, 4 * WINDOW)
+    wide = 2 * HEAD
+    states = poles.shape[2]
+
+    def whole(value):
+        return pl.BlockSpec(value.shape, lambda t: (0,) * value.ndim)
+
+    def by_rows(width):
+        return pl.BlockSpec((block, width), lambda t: (t, 0))
+
+    front = ((wide - drive.shape[1], 0), (0, 0))
+    drive = jnp.pad(drive[0], front)
+    readout = jnp.pad(readout[0], front)
+    skip = jnp.pad(skip_gain, front[0]).reshape(1, wide)
     return pl.pallas_call(
-        flow_kernel,
-        grid=(rows // chunk,),
+        layer_kernel,
+        grid=(rows // block,),
         in_specs=[
-            pl.BlockSpec((chunk, channels), lambda t: (t, 0)),
-            pl.BlockSpec((1, channels, wide), lambda t: (0, 0, 0)),
-            pl.BlockSpec((1, 2, wide // 2), lambda t: (0, 0, 0)),
-            pl.BlockSpec((1, channels, wide), lambda t: (0, 0, 0)),
-            pl.BlockSpec((1, channels), lambda t: (0, 0)),
-        ],
-        out_specs=pl.BlockSpec((chunk, channels), lambda t: (t, 0)),
-        out_shape=jax.ShapeDtypeStruct(inputs.shape, jnp.bfloat16),
-        scratch_shapes=[pltpu.VMEM((2, wide // 2), jnp.float32)],
-    )(inputs, drive, poles, readout, skip_gain.reshape(1, channels))
+            pl.BlockSpec(memory_space=pltpu.SMEM),
+            by_rows(depth),
+            whole(w_in),
+            by_rows(wide),
+            by_rows(wide),
+            whole(drive),
+            whole(poles),
+            whole(readout),
+            whole(skip),
+        ],
+        out_specs=by_rows(wide),
+        out_shape=jax.ShapeDtypeStruct((rows, wide), jnp.bfloat16),
+        scratch_shapes=[
+            pltpu.VMEM((WINDOW, wide), jnp.bfloat16),
+            pltpu.VMEM((WINDOW, wide), jnp.bfloat16),
+            pltpu.VMEM((2, states), jnp.float32),
+        ],
+    )(sink_logit, normed, w_in, cosine, sine, drive, poles, readout, skip)
 
 
 def out_kernel(acts_ref, w_ref, sum_ref):
@@ -400,9 +478,6 @@
         return jnp.repeat(weight.reshape(depth, -1, HEAD), repeats, axis=1)
 
     pieces = (per_device(w_query), per_head(w_key), per_head(w_value), per_device(w_state_in))
-    key_at = pieces[0].shape[2]
-    value_at = key_at + HEAD
-    input_at = value_at + HEAD
     parcels = jnp.concatenate(pieces, axis=2).transpose(1, 0, 2)
     w_in = lax.all_to_all(parcels, "sp", split_axis=0, concat_axis=0, tiled=True)
     w_in = w_in.reshape(devices * depth, parcels.shape[2])
@@ -422,26 +497,13 @@
     poles, drive, readout = state_params(
         decay_rate, rotation, log_step, in_re, in_im, out_re, out_im
     )
-    sums = jnp.dot(normed, w_in, preferred_element_type=jnp.float32)
-    inputs = sums[:, input_at:].astype(jnp.bfloat16)
-    queries, key_rows, value_rows = shape_heads(
-        sums[:, :key_at],
-        sums[:, key_at:value_at],
-        sums[:, value_at:input_at],
-        jnp.arange(rows, dtype=jnp.int32),
-        HEAD,
-    )
-
-    def padded(value):
-        return jnp.pad(value, ((WINDOW, 0), (0, 0))).reshape(WINDOW + rows, 1, HEAD)
-
-    attended = band_attention(
-        queries, padded(key_rows), padded(value_rows), sink_logit, jnp.int32(0), WINDOW
-    )
-    mixed_state = state_flow(inputs, poles, drive, readout, skip_gain, row_count)
-    acts = lax.all_gather(
-        jnp.concatenate([attended, mixed_state], axis=1), everyone, axis=0, tiled=False
-    )
+    frequency = rotary_base ** (-(jnp.arange(HEAD // 2, dtype=jnp.float32) * 2.0 / HEAD))
+    angles = jnp.arange(rows, dtype=jnp.int32).astype(jnp.float32)[:, None] * frequency[None, :]
+    sine_part = jnp.sin(angles)
+    cosine = jnp.tile(jnp.cos(angles), (1, 4))
+    sine = jnp.concatenate([-sine_part, sine_part, -sine_part, sine_part], axis=1)
+    mine = layer(normed, w_in, cosine, sine, sink_logit, poles, drive, readout, skip_gain)
+    acts = lax.all_gather(mine, everyone, axis=0, tiled=False)
     summed = out_project(acts, w_pair)
     projected = lax.all_to_all(summed, everyone, split_axis=0, concat_axis=1, tiled=True)
     projected = projected.astype(jnp.float32)
@@ -541,11 +603,11 @@
     devices = lax.axis_size("sp")
     heads = w_query.shape[1] // HEAD
     groups = others[5].shape[0]
-    group_size = w_query.shape[1] // w_key.shape[1]
     fits = (
-        heads % devices == 0
+        heads == devices
         and groups % devices == 0
-        and group_size % max(heads // devices, 1) == 0
+        and others[1].shape[1] == w_query.shape[1]
+        and tokens.shape[0] % WINDOW == 0
         and tokens.shape[0] % (8 * lax.axis_size("tp")) == 0
     )
     return (by_heads if fits else by_tokens)(tokens, norm_gain, w_query, w_key, *others)

time: 352 us -> 343 us (0.974)
  Pallas kernels: 25.1 us -> 41.7 us
  waiting for transfers between devices: 225 us -> 211 us
  matrix products: 13.4 us -> 0 us
    pallas_call x1, Pallas kernels: 13.6 us -> 30.3 us  [layer(): pl.pallas_call(layer_kernel, grid=(rows // block,), in_specs=[pl.BlockSpe...]
    all_to_all x1, waiting for transfers between devices: 57.7 us -> 42.9 us  [by_heads(): lax.all_to_all(parcels, 'sp', split_axis=0, concat_axis=0, tiled=True)]
    dot_general x3 -> x0, matrix products: 13.4 us -> none  [the longest x1 8.75 us: by_heads(): sums = jnp.dot(normed, w_in, preferred_element_type=jnp.float32)]
    neg x0 -> x1, other arithmetic: none -> 5.55 us  [by_heads(): -sine_part]
    another operation x0 -> x2, local copies, waits for them, and re-layouts: none -> 3.62 us  [by_heads(): cosine = jnp.tile(jnp.cos(angles), (1, 4))]
    unnamed x3 -> x1, other arithmetic: 9.21 us -> 6.78 us
  transfers between devices with their start and end apart: 3 -> 3, of which waited for: 3 -> 3; matrix products, arithmetic and copies ran while one was open for 7% -> 12% of each run, Pallas kernels for 0% -> 0%
where the time goes in v2:
time: 343 us; the launch traced here: 342 us
  waiting for transfers between devices  211 us (62%)
  Pallas kernels  41.7 us (12%)
  other arithmetic  25.8 us (8%)
  blocking collectives  23 us (7%)
  local copies, waits for them, and re-layouts  19 us (6%)
  between operations  13.7 us (4%)
  starting transfers between devices  8.42 us (2%)
    all_gather x1, waiting for transfers between devices, by_heads(): acts = lax.all_gather(mine, everyone, axis=0, tiled=False)  94.9 us
    all_gather x1, waiting for transfers between devices, by_heads(): lax.all_gather(normalize(own_part(tokens, 'tp'), norm_gain), everyone, ax...  72.9 us
    all_to_all x1, waiting for transfers between devices, by_heads(): lax.all_to_all(parcels, 'sp', split_axis=0, concat_axis=0, tiled=True)  42.9 us
    pallas_call x1, Pallas kernels, layer(): pl.pallas_call(layer_kernel, grid=(rows // block,), in_specs=[pl.BlockSpe...  30.3 us
    all_to_all x1, blocking collectives, by_heads(): lax.all_to_all(summed, everyone, split_axis=0, concat_axis=1, tiled=True)  18.4 us
    pallas_call x1, Pallas kernels, out_project(): pl.pallas_call(out_kernel, grid=(rows // block,), in_specs=[pl.BlockSpec(...  11.4 us
    all_to_all x1, starting transfers between devices, by_heads(): lax.all_to_all(parcels, 'sp', split_axis=0, concat_axis=0, tiled=True)  8.34 us
  transfers between devices with their start and end apart: 3, of which 3 were waited for; matrix products, arithmetic and copies ran while one was open for 12% of the time, Pallas kernels for 0%

profile of v2, /device:TPU:0, one launch (start us, length us, event | category | flops | bytes accessed | tf_op | source)
XLA Modules:
  0.0 342.3 jit_solution(7244217240431220286)
XLA Ops:
  6.6 1.3 fusion
  7.9 2.0 fusion.2
  10.8 1.5 maximum_bitcast_fusion
  12.3 8.3 %all-to-all-start = ((bf16[16,256,256]{1,2,0:T(8,128)(2,1)}), bf16[16,256,256]{1,2,0:T(8,128)(2,1)S(1)}, u32[]{:S(2)}, u32[]{:S(2)}) async-start(bf16[16,256,256]{1,2,0:T(8,128)(2,1)} %maximum_bitcast_fusion), calls=%async_computation | async-start | bytes 4194304 | tf_op jit(solution)/shard_map/all_to_all | solution.py:482
  20.7 5.5 %fusion.6 = (f32[2048,32]{1,0:T(8,128)S(1)}, f32[2048,32]{1,0:T(8,128)}, f32[2048,32]{1,0:T(8,128)}) fusion(f32[32]{0:T(128)S(1)} %negate_power_fusion, f32[2048]{0:T(1024)S(1)} %iota_convert_fusion), kind=kLoop, calls=%fused_computation.16 | loop fusion | flops 131072 | bytes 794752 | tf_op jit(solution)/shard_map/neg | solution.py:504
  26.3 1.5 copy.62
  27.8 1.1 tile.49
  28.9 2.5 copy.63.cosine_ref
  31.4 0.8 dynamic-slice_negate_fusion
  32.5 0.8 add_divide_fusion
  33.5 0.7 subtract_divide_fusion
  34.2 0.8 multiply_subtract_fusion
  35.6 0.7 pad.11.drive_ref
  36.4 0.7 pad.12.out_ref
  37.7 0.8 dynamic_slice.39
  38.5 0.7 pad_bitcast_fusion.skip_ref
  39.7 3.4 pad_maximum_fusion.sine_ref
  43.1 42.9 %all-to-all-done = bf16[16,256,256]{1,2,0:T(8,128)(2,1)S(1)} async-done(((bf16[16,256,256]{1,2,0:T(8,128)(2,1)}), bf16[16,256,256]{1,2,0:T(8,128)(2,1)S(1)}, u32[]{:S(2)}, u32[]{:S(2)}) %all-to-all-start) | async-done | bytes 2097184 | tf_op jit(solution)/shard_map/all_to_all | solution.py:482
  86.1 2.4 copy.60
  88.4 72.9 %all-gather.4.cloned.1.call-done.normed_ref = bf16[2048,4096]{1,0:T(8,128)(2,1)} async-done(((bf16[64,4096]{1,0:T(8,128)(2,1)}), bf16[2048,4096]{1,0:T(8,128)(2,1)}) %all-gather.4.cloned.1.call-update) | async-done | bytes 16777232 | tf_op jit(solution)/shard_map/all_gather | solution.py:467
  161.3 30.3 %shard_map.172 = bf16[2048,128]{1,0:T(8,128)(2,1)} custom-call(f32[1]{0:T(128)} %dynamic_slice.30.sink_ref, bf16[2048,4096]{1,0:T(8,128)(2,1)} %all-gather.4.cloned.1.call-done.normed_ref, bf16[4096,256]{1,0:T(8,128)(2,1)} %bitcast.46, f32[2048,128]{1,0:T(8,128)} %copy.63.cosine_ref, f32[2048,128]{1,0:T(8,128)} %pad_maximum_fusion.sine_ref, ...), custom_call_target="tpu_custom_call" | custom-call | tf_op jit(solution)/shard_map/pallas_call | solution.py:377
  191.8 2.2 copy.64
  194.5 6.8 %reduce.2 = bf16[256,2048]{1,0:T(8,128)(2,1)S(1)} reduce(bf16[256,1,2048]{2,1,0:T(2,128)(2,1)S(1)} %bitcast.48, bf16[]{:T(256)} %broadcast.642), dimensions={1}, to_apply=%bitcast.42.reduce_sub_computation | reduce | bytes 2097154
  201.3 0.8 reshape.668
  202.1 4.6 %all_to_all.36 = bf16[2,2,131072]{2,1,0:T(2,128)(2,1)S(1)} all-to-all(bf16[2,2,131072]{2,1,0:T(2,128)(2,1)S(1)} %reshape.668), channel_id=1, replica_groups=mesh['sp'=16,'tp'=2] {'tp'}, dimensions={0} | all-to-all | bytes 2097152 | tf_op jit(solution)/shard_map/all_to_all | solution.py:490
  206.7 0.9 reshape.669
  207.6 0.6 copy.67
  208.2 1.3 copy.65
  209.5 94.9 %all-gather.6.cloned.1.call-done = bf16[65536,128]{1,0:T(8,128)(2,1)} async-done(((bf16[2048,128]{1,0:T(8,128)(2,1)}), bf16[65536,128]{1,0:T(8,128)(2,1)}) %all-gather.6.cloned.1.call-update) | async-done | bytes 16777232 | tf_op jit(solution)/shard_map/all_gather | solution.py:506
  304.4 11.4 %shard_map.173 = bf16[2048,128]{1,0:T(8,128)(2,1)} custom-call(bf16[32,2048,128]{2,1,0:T(8,128)(2,1)} %bitcast.45, bf16[2,2048,128]{2,1,0:T(8,128)(2,1)} %bitcast.49), custom_call_target="tpu_custom_call" | custom-call | tf_op jit(solution)/shard_map/pallas_call | solution.py:418
  315.8 18.4 %all_to_all.37 = bf16[32,64,128]{2,1,0:T(8,128)(2,1)S(1)} all-to-all(bf16[32,64,128]{2,1,0:T(8,128)(2,1)} %bitcast.53), channel_id=1, replica_groups=mesh['sp'=16,'tp'=2] {'sp','tp'}, dimensions={0} | all-to-all | bytes 1048576 | tf_op jit(solution)/shard_map/all_to_all | solution.py:508
  334.5 1.0 fusion.5
  (55 shorter events, 3.9 us)
Async XLA Ops:
  6.5 3.5 %copy-start = (bf16[256,1024]{1,0:T(8,128)(2,1)S(1)}, bf16[256,1024]{1,0:T(8,128)(2,1)}, u32[]{:S(2)}) copy-start(bf16[256,1024]{1,0:T(8,128)(2,1)} %param.23) | copy-start | bytes 1572868
  6.5 3.7 %copy-start.4 = (bf16[256,256]{1,0:T(8,128)(2,1)S(1)}, bf16[256,256]{1,0:T(8,128)(2,1)}, u32[]{:S(2)}) copy-start(bf16[256,256]{1,0:T(8,128)(2,1)} %param.22) | copy-start | bytes 393220
  6.5 3.8 %copy-start.5 = (bf16[256,256]{1,0:T(8,128)(2,1)S(1)}, bf16[256,256]{1,0:T(8,128)(2,1)}, u32[]{:S(2)}) copy-start(bf16[256,256]{1,0:T(8,128)(2,1)} %param.21) | copy-start | bytes 393220
  6.5 3.9 %copy-start.1 = (bf16[256,1024]{1,0:T(8,128)(2,1)S(1)}, bf16[256,1024]{1,0:T(8,128)(2,1)}, u32[]{:S(2)}) copy-start(bf16[256,1024]{1,0:T(8,128)(2,1)} %param.20) | copy-start | bytes 1572868
  6.5 154.8 %all-gather.4.cloned.1.call-start = ((), (), s32[]{:S(2)}) async-start(), calls=%async_computation.3 | async-start | bytes 17301504 | tf_op jit(solution)/shard_map/all_gather | solution.py:467
  12.3 73.8 %all-to-all-start = ((bf16[16,256,256]{1,2,0:T(8,128)(2,1)}), bf16[16,256,256]{1,2,0:T(8,128)(2,1)S(1)}, u32[]{:S(2)}, u32[]{:S(2)}) async-start(bf16[16,256,256]{1,2,0:T(8,128)(2,1)} %maximum_bitcast_fusion), calls=%async_computation | async-start | bytes 4194304 | tf_op jit(solution)/shard_map/all_to_all | solution.py:482
  20.7 283.7 %all-gather.6.cloned.1.call-start = ((), (), s32[]{:S(2)}) async-start(), calls=%async_computation.4 | async-start | bytes 17301504 | tf_op jit(solution)/shard_map/all_gather | solution.py:506
  27.8 4.6 %copy-start.7 = (f32[64]{0:T(128)S(1)}, f32[64]{0:T(128)}, u32[]{:S(2)}) copy-start(f32[64]{0:T(128)} %param.27) | copy-start | bytes 772
  31.4 5.7 %copy-start.8 = (f32[16]{0:T(128)S(1)}, f32[16]{0:T(128)}, u32[]{:S(2)}) copy-start(f32[16]{0:T(128)} %param.24) | copy-start | bytes 196
  161.3 30.4 %copy-start.2 = (bf16[1024,256]{1,0:T(8,128)(2,1)S(1)}, bf16[1024,256]{1,0:T(8,128)(2,1)}, u32[]{:S(2)}) copy-start(bf16[1024,256]{1,0:T(8,128)(2,1)} %param.34) | copy-start | bytes 1572868
  161.3 30.4 %copy-start.3 = (bf16[1024,256]{1,0:T(8,128)(2,1)S(1)}, bf16[1024,256]{1,0:T(8,128)(2,1)}, u32[]{:S(2)}) copy-start(bf16[1024,256]{1,0:T(8,128)(2,1)} %param.33) | copy-start | bytes 1572868
  304.4 30.1 %copy-start.6 = (f32[4096]{0:T(1024)S(1)}, f32[4096]{0:T(1024)}, u32[]{:S(2)}) copy-start(f32[4096]{0:T(1024)} %param.35) | copy-start | bytes 49156
Sparse Core Ops, SparseCore 0:
  10.2 151.0 all-gather.3
  191.8 112.5 all-gather.5
